TPU v7x, 512 devices: a whole 4x8x8 slice. The times are simulated.
512 devices in a mesh: sp: 64 (over z, y), dp: 8 (over x, core).
Axes of the slice: x: 4, y: 8, z: 8, core: 2. Of those that a mesh axis runs over, the one named last changes fastest.
Arguments:
- inputs: bfloat16 [8, 8192, 2048], P('dp', 'sp'), may hold values from -6 to 6
- conv_weight: bfloat16 [4, 2048], replicated, may hold values from -3 to 3
- gate_weight: bfloat16 [2, 8, 256, 256], P(None, 'dp'), may hold values from -0.375 to 0.375
- rate_param: float32 [2048], replicated, may hold values from 4 to 12.5
- pace: float32 [8, 8192], P('dp'), may hold values from 0.5 to 30000
Outputs:
- recurrent: bfloat16 [8, 8192, 2048], P('dp', 'sp')
All inputs are finite; a program needn't handle non-finite values.
Results may differ from a plain program's by a relative error of at most 0.008.
Values may be sent and summed in bfloat16 or wider, within the bound.
No kernel may reach another device: no remote copies, remote signals or barrier semaphores. Data moves between devices by JAX's collectives and lax.ppermute only.
A program may use at most 128 MiB of HBM per device.

v0:
```python
import jax
import jax.numpy as jnp
from jax import lax
from jax.sharding import Mesh
from jax.sharding import PartitionSpec as P

HEADS = 8
BLOCK = 256
CONV = 4
DP = ("dp_0", "dp_1")
gate_power = 8.0


def passed_along(array, axis, by):
    devices = lax.axis_size(axis)
    pairs = [(i, i + by) for i in range(devices) if 0 <= i + by < devices]
    return lax.ppermute(array, axis, pairs)


def piece_ends(length, count):
    unit = 8 if length >= 8 * count else 1
    return [length // unit * k // count * unit for k in range(1, count)]


def gather_in_order(array, axes, sequence):
    pieces = array[None]
    for k in sequence:
        pieces = lax.all_gather(pieces, axes[k], axis=0, tiled=True)
    block = [lax.axis_size(axes[k]) for k in reversed(sequence)]
    pieces = pieces.reshape(*block, *array.shape)
    turned = sorted(range(len(sequence)), key=lambda place: sequence[len(sequence) - 1 - place])
    return pieces.transpose(*turned, *range(len(sequence), pieces.ndim)).reshape(-1, *array.shape)


def joined_along(pieces, dim):
    lengths = list(pieces.shape[1:])
    lengths[dim] *= pieces.shape[0]
    return jnp.moveaxis(pieces, 0, dim).reshape(lengths)


def gather_all_axes(array, axes, dim):
    widest = max(range(max(1, array.ndim - 1)), key=lambda d: array.shape[d])
    count, outs = (len(axes), [])
    for leading, section in enumerate(
        jnp.split(array, piece_ends(array.shape[widest], count), axis=widest)
    ):
        if section.size:
            sequence = [(leading - k) % count for k in range(count)]
            outs.append(gather_in_order(section, axes, sequence))
    return joined_along(jnp.concatenate(outs, axis=widest + 1), dim)


def from_everyone(array, axis):
    copies = jnp.broadcast_to(array, (lax.axis_size(axis), *array.shape))
    return lax.all_to_all(copies, axis, split_axis=0, concat_axis=0, tiled=True)


def gathered_once(array, axis):
    leaves = jax.tree.leaves(array)
    sequence = sorted(range(len(leaves)), key=lambda k: -leaves[k].size)
    width = (1, *leaves[sequence[0]].shape)[-1]
    lines = [
        jnp.pad(leaves[k].reshape(-1), (0, -leaves[k].size % width)).reshape(-1, width)
        for k in sequence
    ]
    both, at, found = (from_everyone(jnp.concatenate(lines), axis), 0, {})
    for k, line in zip(sequence, lines):
        section = both[:, at : at + len(line)].reshape(len(both), -1)
        found[k] = section[:, : leaves[k].size].reshape(-1, *leaves[k].shape)
        at += len(line)
    numbers = iter(range(len(leaves)))
    return jax.tree.map(lambda _: found[next(numbers)], array)


def combined_pairwise(pieces, combine):
    while len(jax.tree.leaves(pieces)[0]) > 1:
        pieces = jax.vmap(combine)(
            *(jax.tree.map(lambda part: part[side::2], pieces) for side in (0, 1))
        )
    return jax.tree.map(lambda part: part[0], pieces)


def prefix(array, axis, combine, identity):
    devices, here = (lax.axis_size(axis), lax.axis_index(axis))
    passed = jnp.arange(devices) < here

    def kept(part, zero, own):
        part = jnp.where(
            passed.reshape(-1, *(1 for _ in own.shape)), part, jnp.asarray(zero, own.dtype)
        )
        return part

    pieces = gathered_once(array, axis)
    return combined_pairwise(jax.tree.map(kept, pieces, identity, array), combine)


def combine(earlier, later):
    decay_e, state_e = earlier
    decay_l, state_l = later
    return (decay_e * decay_l, decay_l * state_e + state_l)


def lru_terms(pre_recur, pre_input, values, rate_col, pace_col):
    recur_gate = jax.nn.sigmoid(pre_recur.astype(jnp.float32))
    input_gate = jax.nn.sigmoid(pre_input.astype(jnp.float32))
    log_decay = -gate_power * pace_col * recur_gate * jax.nn.softplus(-rate_col)
    decay = jnp.exp(log_decay)
    drive = jnp.sqrt(-jnp.expm1(2.0 * log_decay)) * input_gate * values.astype(jnp.float32)
    return (decay, drive)


def body(inputs, conv_weight, gate_weight, rate_param, pace):
    own_rows = inputs[0].T
    width = own_rows.shape[0]
    count = own_rows.shape[1]
    earlier = passed_along(own_rows[:, count - (CONV - 1) :], "sp", 1)
    padded = jnp.concatenate([earlier, own_rows], axis=1).astype(jnp.float32)
    conv_taps = conv_weight.astype(jnp.float32)
    conv_out = jnp.zeros((width, count), jnp.float32)
    for tap in range(CONV):
        conv_out = conv_out + conv_taps[tap][:, None] * padded[:, tap : tap + count]
    conv_out = conv_out.astype(jnp.bfloat16)
    by_head = conv_out.reshape(HEADS, BLOCK, count)
    preact = (
        jnp.einsum(
            "hit,ghij->ghjt",
            by_head,
            gather_all_axes(gate_weight, DP, 1),
            preferred_element_type=jnp.float32,
        )
        .astype(jnp.bfloat16)
        .reshape(2, width, count)
    )
    own_pace = lax.dynamic_slice_in_dim(pace[0], lax.axis_index("sp") * count, count)
    decay, drive = lru_terms(preact[0], preact[1], conv_out, rate_param[:, None], own_pace[None, :])
    decay_run, state = lax.associative_scan(combine, (decay, drive), axis=1)
    identity = (jnp.ones((width,), jnp.float32), jnp.zeros((width,), jnp.float32))
    _, carried = prefix((decay_run[:, -1], state[:, -1]), "sp", combine, identity)
    result = (state + decay_run * carried[:, None]).astype(jnp.bfloat16)
    return result.T[None]


def solution(mesh):
    finer = Mesh(mesh.devices.reshape(mesh.shape["sp"], 4, 2), ("sp", "dp_0", "dp_1"))
    in_specs = (P(DP, "sp", None), P(), P(None, DP, None, None), P(), P(DP, None))
    out_specs = P(DP, "sp", None)
    return jax.shard_map(body, mesh=finer, in_specs=in_specs, out_specs=out_specs, check_vma=False)
```

profile of v0, /device:TPU:8, one launch (start us, length us, event | category | flops | bytes accessed | tf_op | source)
XLA Modules:
  0.0 180.7 jit_solution(7112969151282541759)
XLA Ops:
  7.6 13.9 %all-gather = bf16[8,1,128,256]{3,2,1,0:T(8,128)(2,1)} all-gather(bf16[2,1,128,256]{3,2,1,0:T(8,128)(2,1)S(1)} %get-tuple-element.21), channel_id=2, replica_groups=mesh['sp'=64,'dp_0'=4,'dp_1'=2] {'dp_0'}, dimensions={0}, use_global_device_ids=true | all-gather | bytes 655360 | tf_op jit(solution)/shard_map/all_gather | solution.py:28
  21.5 2.1 %all-gather.1 = bf16[4,1,128,256]{3,2,1,0:T(8,128)(2,1)} all-gather(bf16[2,1,128,256]{3,2,1,0:T(8,128)(2,1)S(1)} %get-tuple-element.22), channel_id=3, replica_groups=mesh['sp'=64,'dp_0'=4,'dp_1'=2] {'dp_1'}, dimensions={0}, use_global_device_ids=true | all-gather | bytes 393216 | tf_op jit(solution)/shard_map/all_gather | solution.py:28
  23.7 3.5 %collective-permute-start = (bf16[2048,3]{0,1:T(4,128)(2,1)S(1)}, bf16[2048,3]{0,1:T(4,128)(2,1)S(1)}, u32[]{:S(2)}, u32[]{:S(2)}) collective-permute-start(bf16[2048,3]{0,1:T(4,128)(2,1)S(1)} %slice.422), channel_id=1, source_target_pairs={{0,8},{8,16},{16,24},{24,32},{32,40},{40,48},{48,56},{56,64},{64,7... | collective-permute-start | bytes 36872 | tf_op jit(solution)/shard_map/ppermute | solution.py:17
  28.0 4.3 %collective-permute-done = bf16[2048,3]{0,1:T(4,128)(2,1)S(1)} collective-permute-done((bf16[2048,3]{0,1:T(4,128)(2,1)S(1)}, bf16[2048,3]{0,1:T(4,128)(2,1)S(1)}, u32[]{:S(2)}, u32[]{:S(2)}) %collective-permute-start) | collective-permute-done | bytes 12320 | tf_op jit(solution)/shard_map/ppermute | solution.py:17
  33.9 9.5 %all-gather.5.cloned.1.call-done = bf16[8,2,1,128,256]{4,3,2,1,0:T(8,128)(2,1)} async-done(((bf16[4,2,1,128,256]{4,3,2,1,0:T(8,128)(2,1)}), bf16[8,2,1,128,256]{4,3,2,1,0:T(8,128)(2,1)}) %all-gather.5.cloned.1.call-update) | async-done | bytes 1048592 | tf_op jit(solution)/shard_map/all_gather | solution.py:28
  43.4 1.6 copy.16
  45.1 31.2 %all-gather.7.cloned.1.call-done = bf16[8,2,1,128,256]{4,3,2,1,0:T(8,128)(2,1)} async-done(((bf16[2,2,1,128,256]{4,3,2,1,0:T(8,128)(2,1)}), bf16[8,2,1,128,256]{4,3,2,1,0:T(8,128)(2,1)}) %all-gather.7.cloned.1.call-update) | async-done | bytes 1048592 | tf_op jit(solution)/shard_map/all_gather | solution.py:28
  76.3 1.6 copy.18
  77.9 1.7 fusion.4
  82.9 2.8 %convert_multiply_fusion = (f32[2048,128]{0,1:T(8,128)S(1)}, f32[2048,128]{0,1:T(8,128)S(1)}) fusion(f32[2048,128]{0,1:T(8,128)} %copy.21, f32[2048,128]{0,1:T(8,128)} %copy.20, f32[2048]{0:T(1024)S(1)} %compare_select_fusion, f32[128]{0:T(128)S(1)} %multiply_bitcast_fusion, f32[2048,131]{0,1:T(8,128)S(1)} %maximum_convert_fusion, f32[2048]{0:T(1024)S(1)} %bitcast.69, ...), kind=kLoop, calls=%fused_computation.15 | loop fusion | flops 3932160 | bytes 8430080 | tf_op jit(solution)/shard_map/mul | solution.py:108
  85.7 1.5 slice.380
  93.1 1.5 slice.331
  102.7 2.1 %pad.99 = f32[2048,128]{0,1:T(8,128)S(1)} pad(f32[2048,64]{0,1:T(8,128)} %add.213, f32[]{:T(128)} %constant.8.clone.1), padding=0_0_0x1_0_1 | pad | bytes 1572868 | tf_op jit(solution)/shard_map/pad | solution.py:136
  104.8 4.6 %pad.113 = f32[2048,128]{0,1:T(8,128)} pad(f32[2048,64]{0,1:T(8,128)} %add.221, f32[]{:T(128)} %constant.8.clone.1), padding=0_0_0x1_0_1 | pad | bytes 1572868 | tf_op jit(solution)/shard_map/pad | solution.py:136
  111.9 13.6 %all-to-all-start = ((f32[64,2,2048]{2,1,0:T(2,128)}), f32[64,2,2048]{2,1,0:T(2,128)}, u32[]{:S(2)}, u32[]{:S(2)}) async-start(f32[64,2,2048]{2,1,0:T(2,128)} %broadcast_in_dim.37), calls=%async_computation | async-start | bytes 2097152 | tf_op jit(solution)/shard_map/all_to_all | solution.py:55
  125.5 27.8 %all-to-all-done = f32[64,2,2048]{2,1,0:T(2,128)} async-done(((f32[64,2,2048]{2,1,0:T(2,128)}), f32[64,2,2048]{2,1,0:T(2,128)}, u32[]{:S(2)}, u32[]{:S(2)}) %all-to-all-start) | async-done | bytes 1048608 | tf_op jit(solution)/shard_map/all_to_all | solution.py:55
  153.2 2.6 %fusion.22 = (f32[64,1,2048]{2,1,0:T(1,128)S(1)}, f32[64,1,2048]{2,1,0:T(1,128)S(1)}) fusion(f32[64,2,2048]{2,1,0:T(2,128)} %all-to-all-done), kind=kLoop, calls=%fused_computation.86 | loop fusion | bytes 2097152 | tf_op jit(solution)/shard_map/slice | solution.py:68
  157.2 1.7 slice.398
  158.9 1.7 slice.397
  160.6 1.7 slice.410
  162.3 1.7 slice.409
  164.0 1.9 %fusion.23 = (f32[32,2048]{1,0:T(8,128)}, f32[32,2048]{1,0:T(8,128)S(1)}) fusion(f32[32,2048]{1,0:T(8,128)} %slice.397, f32[32,2048]{1,0:T(8,128)} %slice.398, f32[32,2048]{1,0:T(8,128)} %slice.410, f32[32,2048]{1,0:T(8,128)} %slice.409), kind=kLoop, calls=%fused_computation.87 | loop fusion | flops 196608 | bytes 1572864 | tf_op jit(solution)/shard_map/vmap()/mul | solution.py:100
  166.9 1.6 slice.399
  171.5 2.3 %fusion.10 = bf16[1,128,2048]{2,1,0:T(8,128)(2,1)} fusion(f32[2048,128]{0,1:T(8,128)S(1)} %pad.112, f32[2048,128]{0,1:T(8,128)} %pad.113, f32[2048,128]{0,1:T(8,128)S(1)} %pad.98, f32[2048,128]{0,1:T(8,128)S(1)} %pad.99, f32[2048]{0:T(1024)S(1)} %bitcast.70), kind=kLoop, calls=%fused_computation.21 | loop fusion | flops 1310720 | bytes 4726784 | tf_op jit(solution)/shard_map/broadcast_in_dim | solution.py:140
  (154 shorter events, 27.6 us)
Async XLA Ops:
  6.5 17.2 %copy-start.4 = (bf16[1,128,2048]{2,1,0:T(8,128)(2,1)S(1)}, bf16[1,128,2048]{2,1,0:T(8,128)(2,1)}, u32[]{:S(2)}) copy-start(bf16[1,128,2048]{2,1,0:T(8,128)(2,1)} %param.5) | copy-start | bytes 1572868
  6.5 20.7 %copy-start.6 = (f32[2048]{0:T(1024)S(1)}, f32[2048]{0:T(1024)}, u32[]{:S(2)}) copy-start(f32[2048]{0:T(1024)} %param.8) | copy-start | bytes 24580
  6.5 20.7 %copy-start.5 = (bf16[4,2048]{1,0:T(4,128)(2,1)S(1)}, bf16[4,2048]{1,0:T(4,128)(2,1)}, u32[]{:S(2)}) copy-start(bf16[4,2048]{1,0:T(4,128)(2,1)} %param.6) | copy-start | bytes 49156
  6.5 36.9 %all-gather.5.cloned.1.call-start = ((), (), s32[]{:S(2)}) async-start(), calls=%async_computation.1 | async-start | bytes 1572864 | tf_op jit(solution)/shard_map/all_gather | solution.py:28
  21.5 54.8 %all-gather.7.cloned.1.call-start = ((), (), s32[]{:S(2)}) async-start(), calls=%async_computation.2 | async-start | bytes 1310720 | tf_op jit(solution)/shard_map/all_gather | solution.py:28
  23.7 8.6 %collective-permute-start = (bf16[2048,3]{0,1:T(4,128)(2,1)S(1)}, bf16[2048,3]{0,1:T(4,128)(2,1)S(1)}, u32[]{:S(2)}, u32[]{:S(2)}) collective-permute-start(bf16[2048,3]{0,1:T(4,128)(2,1)S(1)} %slice.422), channel_id=1, source_target_pairs={{0,8},{8,16},{16,24},{24,32},{32,40},{40,48},{48,56},{56,64},{64,7... | collective-permute-start | bytes 36872 | tf_op jit(solution)/shard_map/ppermute | solution.py:17
  91.6 3.0 %copy-start = (f32[2048,64]{0,1:T(8,128)S(1)}, f32[2048,64]{0,1:T(8,128)}, u32[]{:S(2)}) copy-start(f32[2048,64]{0,1:T(8,128)} %slice.334) | copy-start | bytes 1572868
  91.6 3.0 %copy-start.1 = (f32[2048,64]{0,1:T(8,128)S(1)}, f32[2048,64]{0,1:T(8,128)}, u32[]{:S(2)}) copy-start(f32[2048,64]{0,1:T(8,128)} %slice.333) | copy-start | bytes 1572868
  100.7 1.2 copy-start.2
  100.7 1.4 copy-start.3
  111.9 41.4 %all-to-all-start = ((f32[64,2,2048]{2,1,0:T(2,128)}), f32[64,2,2048]{2,1,0:T(2,128)}, u32[]{:S(2)}, u32[]{:S(2)}) async-start(f32[64,2,2048]{2,1,0:T(2,128)} %broadcast_in_dim.37), calls=%async_computation | async-start | bytes 2097152 | tf_op jit(solution)/shard_map/all_to_all | solution.py:55
Sparse Core Ops, SparseCore 0:
  21.6 21.7 all-gather.4
  45.5 30.7 all-gather.6
where the time goes:
time: 182 us; the launch traced here: 181 us
  waiting for transfers between devices  72.9 us (40%)
  local copies, waits for them, and re-layouts  42.2 us (23%)
  starting transfers between devices  17.1 us (9%)
  other arithmetic  16.5 us (9%)
  blocking collectives  16 us (9%)
  between operations  14.2 us (8%)
    all_gather x2, waiting for transfers between devices, gather_in_order(): pieces = lax.all_gather(pieces, axes[k], axis=0, tiled=True)  40.8 us
    all_to_all x1, waiting for transfers between devices, from_everyone(): return lax.all_to_all(copies, axis, split_axis=0, concat_axis=0, tiled=True)  27.8 us
    all_gather x2, blocking collectives, gather_in_order(): pieces = lax.all_gather(pieces, axes[k], axis=0, tiled=True)  16 us
    all_to_all x1, starting transfers between devices, from_everyone(): return lax.all_to_all(copies, axis, split_axis=0, concat_axis=0, tiled=True)  13.6 us
    slice x20, local copies, waits for them, and re-layouts, combined_pairwise(): part[side::2]  11.1 us
    slice x44, local copies, waits for them, and re-layouts, body(): decay_run, state = lax.associative_scan(combine, (decay, drive), axis=1)  10.8 us
    pad x24, local copies, waits for them, and re-layouts, body(): decay_run, state = lax.associative_scan(combine, (decay, drive), axis=1)  7.74 us
    ppermute x1, waiting for transfers between devices, passed_along(): return lax.ppermute(array, axis, pairs)  4.33 us
  transfers between devices with their start and end apart: 4, of which 4 were waited for; matrix products, arithmetic and copies ran while one was open for 2% of the time, Pallas kernels for 0%

commit v1 on v0

--- a/solution.py
+++ b/solution.py
@@ -3,6 +3,7 @@
 from jax import lax
 from jax.sharding import Mesh
 from jax.sharding import PartitionSpec as P
+from jax.lax import all_to_all, axis_size
 
 HEADS = 8
 BLOCK = 256
@@ -25,7 +26,11 @@
 def gather_in_order(array, axes, sequence):
     pieces = array[None]
     for k in sequence:
-        pieces = lax.all_gather(pieces, axes[k], axis=0, tiled=True)
+        arr = axes[k]
+        pieces = jnp.concatenate(
+            all_to_all(jnp.stack([pieces for _ in range(axis_size(arr))], axis=0), arr, 0, 0),
+            axis=0,
+        )
     block = [lax.axis_size(axes[k]) for k in reversed(sequence)]
     pieces = pieces.reshape(*block, *array.shape)
     turned = sorted(range(len(sequence)), key=lambda place: sequence[len(sequence) - 1 - place])

time: 182 us -> 153 us (0.84)
  waiting for transfers between devices: 72.9 us -> 53.1 us
  starting transfers between devices: 17.1 us -> 31.5 us
  between operations: 14.2 us -> 0.84 us
  blocking collectives: 16 us -> 4.58 us
    all_gather x2 -> x0, waiting for transfers between devices: 40.8 us -> none  [gather_in_order(): pieces = lax.all_gather(pieces, axes[k], axis=0, tiled=True)]
    all_to_all x0 -> x3, waiting for transfers between devices: none -> 24.3 us  [gather_in_order(): all_to_all(jnp.stack([pieces for _ in range(axis_size(arr))], axis=0), ar...]
    all_gather x2 -> x0, blocking collectives: 16 us -> none  [gather_in_order(): pieces = lax.all_gather(pieces, axes[k], axis=0, tiled=True)]
    all_to_all x0 -> x3, starting transfers between devices: none -> 12.1 us  [gather_in_order(): all_to_all(jnp.stack([pieces for _ in range(axis_size(arr))], axis=0), ar...]
    all_to_all x0 -> x1, blocking collectives: none -> 4.58 us  [gather_in_order(): all_to_all(jnp.stack([pieces for _ in range(axis_size(arr))], axis=0), ar...]
    ppermute x1, waiting for transfers between devices: 4.33 us -> 0.01 us  [passed_along(): return lax.ppermute(array, axis, pairs)]
    all_to_all x1, starting transfers between devices: 13.6 us -> 15.9 us  [from_everyone(): return lax.all_to_all(copies, axis, split_axis=0, concat_axis=0, tiled=True)]
    another operation x0 -> x3, local copies, waits for them, and re-layouts: none -> 2.2 us  [gather_in_order(): jnp.stack([pieces for _ in range(axis_size(arr))], axis=0)]
  transfers between devices with their start and end apart: 4 -> 5, of which waited for: 4 -> 4; matrix products, arithmetic and copies ran while one was open for 2% -> 4% of each run, Pallas kernels for 0% -> 0%
where the time goes in v1:
time: 153 us; the launch traced here: 151 us
  waiting for transfers between devices  53.1 us (35%)
  local copies, waits for them, and re-layouts  42.1 us (28%)
  starting transfers between devices  31.5 us (21%)
  other arithmetic  17.3 us (11%)
  blocking collectives  4.58 us (3%)
  matrix products  2.06 us (1%)
    all_to_all x1, waiting for transfers between devices, from_everyone(): return lax.all_to_all(copies, axis, split_axis=0, concat_axis=0, tiled=True)  28.8 us
    all_to_all x3, waiting for transfers between devices, gather_in_order(): all_to_all(jnp.stack([pieces for _ in range(axis_size(arr))], axis=0), ar...  24.3 us
    all_to_all x1, starting transfers between devices, from_everyone(): return lax.all_to_all(copies, axis, split_axis=0, concat_axis=0, tiled=True)  15.9 us
    all_to_all x3, starting transfers between devices, gather_in_order(): all_to_all(jnp.stack([pieces for _ in range(axis_size(arr))], axis=0), ar...  12.1 us
    slice x20, local copies, waits for them, and re-layouts, combined_pairwise(): part[side::2]  11.1 us
    slice x44, local copies, waits for them, and re-layouts, body(): decay_run, state = lax.associative_scan(combine, (decay, drive), axis=1)  10.8 us
    pad x24, local copies, waits for them, and re-layouts, body(): decay_run, state = lax.associative_scan(combine, (decay, drive), axis=1)  7.74 us
    all_to_all x1, blocking collectives, gather_in_order(): all_to_all(jnp.stack([pieces for _ in range(axis_size(arr))], axis=0), ar...  4.58 us
  transfers between devices with their start and end apart: 5, of which 4 were waited for; matrix products, arithmetic and copies ran while one was open for 4% of the time, Pallas kernels for 0%

profile of v1, /device:TPU:8, one launch (start us, length us, event | category | flops | bytes accessed | tf_op | source)
XLA Modules:
  0.0 151.5 jit_solution(12761005664986415331)
XLA Ops:
  0.8 3.5 %collective-permute-start = (bf16[2048,3]{0,1:T(4,128)(2,1)S(1)}, bf16[2048,3]{0,1:T(4,128)(2,1)S(1)}, u32[]{:S(2)}, u32[]{:S(2)}) collective-permute-start(bf16[2048,3]{0,1:T(4,128)(2,1)S(1)} %slice.422), channel_id=1, source_target_pairs={{0,8},{8,16},{16,24},{24,32},{32,40},{40,48},{48,56},{56,64},{64,7... | collective-permute-start | bytes 36872 | tf_op jit(solution)/shard_map/ppermute | solution.py:18
  6.0 3.4 %all-to-all-start.2 = ((bf16[2,1,2,1,128,256]{5,4,2,3,1,0:T(8,128)(2,1)}), bf16[2,1,2,1,128,256]{5,4,2,3,1,0:T(8,128)(2,1)S(1)}, u32[]{:S(2)}, u32[]{:S(2)}) async-start(bf16[2,1,2,1,128,256]{5,4,2,3,1,0:T(8,128)(2,1)} %pad_maximum_fusion.3), calls=%async_computation.2 | async-start | bytes 524288 | tf_op jit(solution)/shard_map/all_to_all | solution.py:31
  11.9 4.3 %all-to-all-start = ((bf16[4,1,2,1,128,256]{4,5,2,3,1,0:T(8,128)(2,1)}), bf16[4,1,2,1,128,256]{4,5,2,3,1,0:T(8,128)(2,1)S(1)}, u32[]{:S(2)}, u32[]{:S(2)}) async-start(bf16[4,1,2,1,128,256]{4,5,2,3,1,0:T(8,128)(2,1)} %stack.12), calls=%async_computation | async-start | bytes 1048576 | tf_op jit(solution)/shard_map/all_to_all | solution.py:31
  16.4 9.6 %all-to-all-done = bf16[4,1,2,1,128,256]{4,5,2,3,1,0:T(8,128)(2,1)S(1)} async-done(((bf16[4,1,2,1,128,256]{4,5,2,3,1,0:T(8,128)(2,1)}), bf16[4,1,2,1,128,256]{4,5,2,3,1,0:T(8,128)(2,1)S(1)}, u32[]{:S(2)}, u32[]{:S(2)}) %all-to-all-start) | async-done | bytes 524320 | tf_op jit(solution)/shard_map/all_to_all | solution.py:31
  26.0 4.6 %all_to_all.25 = bf16[2,4,2,1,128,256]{4,5,2,1,3,0:T(8,128)(2,1)S(1)} all-to-all(bf16[2,4,2,1,128,256]{4,5,2,1,3,0:T(8,128)(2,1)S(1)} %pad_maximum_fusion), channel_id=1, replica_groups=mesh['sp'=64,'dp_0'=4,'dp_1'=2] {'dp_1'}, dimensions={0} | all-to-all | bytes 2097152 | tf_op jit(solution)/shard_map/all_to_all | solution.py:31
  31.8 4.4 %all-to-all-start.3 = ((bf16[4,2,2,1,128,256]{4,5,2,1,3,0:T(8,128)(2,1)}), bf16[4,2,2,1,128,256]{4,5,2,1,3,0:T(8,128)(2,1)}, u32[]{:S(2)}, u32[]{:S(2)}) async-start(bf16[4,2,2,1,128,256]{4,5,2,1,3,0:T(8,128)(2,1)} %stack.15), calls=%async_computation.3 | async-start | bytes 2097152 | tf_op jit(solution)/shard_map/all_to_all | solution.py:31
  38.6 13.3 %all-to-all-done.3 = bf16[4,2,2,1,128,256]{4,5,2,1,3,0:T(8,128)(2,1)} async-done(((bf16[4,2,2,1,128,256]{4,5,2,1,3,0:T(8,128)(2,1)}), bf16[4,2,2,1,128,256]{4,5,2,1,3,0:T(8,128)(2,1)}, u32[]{:S(2)}, u32[]{:S(2)}) %all-to-all-start.3) | async-done | bytes 1048608 | tf_op jit(solution)/shard_map/all_to_all | solution.py:31
  51.9 2.1 %fusion.4 = bf16[2,8,256,128]{3,2,0,1:T(8,128)(2,1)S(1)} fusion(bf16[8,256,128,1]{2,1,3,0:T(8,128)(2,1)} %bitcast.60, bf16[8,2,1,128,256]{3,4,1,0,2:T(8,128)(2,1)} %bitcast.7, bf16[8,2,1,128,256]{3,4,1,0,2:T(8,128)(2,1)S(1)} %bitcast.56), kind=kOutput, calls=%fused_computation.5 | convolution fusion | flops 273154048 | bytes 3670016 | tf_op jit(solution)/shard_map/hit,ghij->ghjt/dot_general | solution.py:130
  57.2 2.8 %convert_multiply_fusion = (f32[2048,128]{0,1:T(8,128)S(1)}, f32[2048,128]{0,1:T(8,128)S(1)}) fusion(f32[2048,128]{0,1:T(8,128)} %copy.16, f32[2048,128]{0,1:T(8,128)} %copy.15, f32[2048]{0:T(1024)S(1)} %compare_select_fusion, f32[128]{0:T(128)S(1)} %multiply_bitcast_fusion, f32[2048,131]{0,1:T(8,128)S(1)} %maximum_convert_fusion, f32[2048]{0:T(1024)S(1)} %bitcast.68, ...), kind=kLoop, calls=%fused_computation.16 | loop fusion | flops 3932160 | bytes 8430080 | tf_op jit(solution)/shard_map/mul | solution.py:113
  60.0 1.5 %slice.380 = f32[2048,63]{0,1:T(8,128)} slice(f32[2048,128]{0,1:T(8,128)S(1)} %get-tuple-element.5), slice={[0:2048:1], [2:128:2]} | slice | bytes 1032192 | tf_op jit(solution)/shard_map/slice | solution.py:141
  67.4 1.5 %slice.331 = f32[2048,63]{0,1:T(8,128)} slice(f32[2048,128]{0,1:T(8,128)S(1)} %get-tuple-element.6), slice={[0:2048:1], [2:128:2]} | slice | bytes 1032192 | tf_op jit(solution)/shard_map/slice | solution.py:141
  77.0 2.1 %pad.99 = f32[2048,128]{0,1:T(8,128)S(1)} pad(f32[2048,64]{0,1:T(8,128)} %add.213, f32[]{:T(128)} %constant.8.clone.1), padding=0_0_0x1_0_1 | pad | bytes 1572868 | tf_op jit(solution)/shard_map/pad | solution.py:141
  79.1 4.6 %pad.113 = f32[2048,128]{0,1:T(8,128)} pad(f32[2048,64]{0,1:T(8,128)} %add.221, f32[]{:T(128)} %constant.8.clone.1), padding=0_0_0x1_0_1 | pad | bytes 1572868 | tf_op jit(solution)/shard_map/pad | solution.py:141
  84.7 1.5 broadcast_in_dim.29
  86.2 15.9 %all-to-all-start.4 = ((f32[64,2,2048]{2,1,0:T(2,128)}), f32[64,2,2048]{2,1,0:T(2,128)}, u32[]{:S(2)}, u32[]{:S(2)}) async-start(f32[64,2,2048]{2,1,0:T(2,128)} %broadcast_in_dim.29), calls=%async_computation.4 | async-start | bytes 2097152 | tf_op jit(solution)/shard_map/all_to_all | solution.py:60
  102.1 28.8 %all-to-all-done.4 = f32[64,2,2048]{2,1,0:T(2,128)} async-done(((f32[64,2,2048]{2,1,0:T(2,128)}), f32[64,2,2048]{2,1,0:T(2,128)}, u32[]{:S(2)}, u32[]{:S(2)}) %all-to-all-start.4) | async-done | bytes 1048608 | tf_op jit(solution)/shard_map/all_to_all | solution.py:60
  130.9 2.6 %fusion.22 = (f32[64,1,2048]{2,1,0:T(1,128)S(1)}, f32[64,1,2048]{2,1,0:T(1,128)S(1)}) fusion(f32[64,2,2048]{2,1,0:T(2,128)} %all-to-all-done.4), kind=kLoop, calls=%fused_computation.90 | loop fusion | bytes 2097152 | tf_op jit(solution)/shard_map/slice | solution.py:73
  134.9 1.7 %slice.398 = f32[32,2048]{1,0:T(8,128)} slice(f32[64,2048]{1,0:T(8,128)} %get-tuple-element.55), slice={[1:64:2], [0:2048:1]} | slice | bytes 524288 | tf_op jit(solution)/shard_map/slice | solution.py:83
  136.6 1.7 %slice.397 = f32[32,2048]{1,0:T(8,128)} slice(f32[64,2048]{1,0:T(8,128)} %get-tuple-element.55), slice={[0:64:2], [0:2048:1]} | slice | bytes 524288 | tf_op jit(solution)/shard_map/slice | solution.py:83
  138.3 1.7 %slice.410 = f32[32,2048]{1,0:T(8,128)} slice(f32[64,2048]{1,0:T(8,128)} %get-tuple-element.56), slice={[1:64:2], [0:2048:1]} | slice | bytes 524288 | tf_op jit(solution)/shard_map/slice | solution.py:83
  140.0 1.7 %slice.409 = f32[32,2048]{1,0:T(8,128)} slice(f32[64,2048]{1,0:T(8,128)} %get-tuple-element.56), slice={[0:64:2], [0:2048:1]} | slice | bytes 524288 | tf_op jit(solution)/shard_map/slice | solution.py:83
  141.7 1.9 %fusion.23 = (f32[32,2048]{1,0:T(8,128)}, f32[32,2048]{1,0:T(8,128)S(1)}) fusion(f32[32,2048]{1,0:T(8,128)} %slice.397, f32[32,2048]{1,0:T(8,128)} %slice.398, f32[32,2048]{1,0:T(8,128)} %slice.410, f32[32,2048]{1,0:T(8,128)} %slice.409), kind=kLoop, calls=%fused_computation.91 | loop fusion | flops 196608 | bytes 1572864 | tf_op jit(solution)/shard_map/vmap()/mul | solution.py:105
  144.6 1.6 %slice.399 = f32[16,2048]{1,0:T(8,128)} slice(f32[32,2048]{1,0:T(8,128)} %get-tuple-element.15), slice={[0:32:2], [0:2048:1]} | slice | bytes 262144 | tf_op jit(solution)/shard_map/slice | solution.py:83
  149.1 2.3 %fusion.10 = bf16[1,128,2048]{2,1,0:T(8,128)(2,1)} fusion(f32[2048,128]{0,1:T(8,128)S(1)} %pad.112, f32[2048,128]{0,1:T(8,128)} %pad.113, f32[2048,128]{0,1:T(8,128)S(1)} %pad.98, f32[2048,128]{0,1:T(8,128)S(1)} %pad.99, f32[2048]{0:T(1024)S(1)} %bitcast.69), kind=kLoop, calls=%fused_computation.22 | loop fusion | flops 1310720 | bytes 4726784 | tf_op jit(solution)/shard_map/broadcast_in_dim | solution.py:145
  (158 shorter events, 31.4 us)
Async XLA Ops:
  0.0 9.5 %copy-start.6 = (f32[2048]{0:T(1024)S(1)}, f32[2048]{0:T(1024)}, u32[]{:S(2)}) copy-start(f32[2048]{0:T(1024)} %param.8) | copy-start | bytes 24580
  0.8 36.0 %collective-permute-start = (bf16[2048,3]{0,1:T(4,128)(2,1)S(1)}, bf16[2048,3]{0,1:T(4,128)(2,1)S(1)}, u32[]{:S(2)}, u32[]{:S(2)}) collective-permute-start(bf16[2048,3]{0,1:T(4,128)(2,1)S(1)} %slice.422), channel_id=1, source_target_pairs={{0,8},{8,16},{16,24},{24,32},{32,40},{40,48},{48,56},{56,64},{64,7... | collective-permute-start | bytes 36872 | tf_op jit(solution)/shard_map/ppermute | solution.py:18
  6.0 5.0 %all-to-all-start.2 = ((bf16[2,1,2,1,128,256]{5,4,2,3,1,0:T(8,128)(2,1)}), bf16[2,1,2,1,128,256]{5,4,2,3,1,0:T(8,128)(2,1)S(1)}, u32[]{:S(2)}, u32[]{:S(2)}) async-start(bf16[2,1,2,1,128,256]{5,4,2,3,1,0:T(8,128)(2,1)} %pad_maximum_fusion.3), calls=%async_computation.2 | async-start | bytes 524288 | tf_op jit(solution)/shard_map/all_to_all | solution.py:31
  9.6 6.7 %copy-start.5 = (bf16[4,2048]{1,0:T(4,128)(2,1)S(1)}, bf16[4,2048]{1,0:T(4,128)(2,1)}, u32[]{:S(2)}) copy-start(bf16[4,2048]{1,0:T(4,128)(2,1)} %param.6) | copy-start | bytes 49156
  11.9 14.1 %all-to-all-start = ((bf16[4,1,2,1,128,256]{4,5,2,3,1,0:T(8,128)(2,1)}), bf16[4,1,2,1,128,256]{4,5,2,3,1,0:T(8,128)(2,1)S(1)}, u32[]{:S(2)}, u32[]{:S(2)}) async-start(bf16[4,1,2,1,128,256]{4,5,2,3,1,0:T(8,128)(2,1)} %stack.12), calls=%async_computation | async-start | bytes 1048576 | tf_op jit(solution)/shard_map/all_to_all | solution.py:31
  31.8 5.1 %copy-start.4 = (bf16[1,128,2048]{2,1,0:T(8,128)(2,1)S(1)}, bf16[1,128,2048]{2,1,0:T(8,128)(2,1)}, u32[]{:S(2)}) copy-start(bf16[1,128,2048]{2,1,0:T(8,128)(2,1)} %param.5) | copy-start | bytes 1572868
  31.8 20.1 %all-to-all-start.3 = ((bf16[4,2,2,1,128,256]{4,5,2,1,3,0:T(8,128)(2,1)}), bf16[4,2,2,1,128,256]{4,5,2,1,3,0:T(8,128)(2,1)}, u32[]{:S(2)}, u32[]{:S(2)}) async-start(bf16[4,2,2,1,128,256]{4,5,2,1,3,0:T(8,128)(2,1)} %stack.15), calls=%async_computation.3 | async-start | bytes 2097152 | tf_op jit(solution)/shard_map/all_to_all | solution.py:31
  65.9 3.0 %copy-start = (f32[2048,64]{0,1:T(8,128)S(1)}, f32[2048,64]{0,1:T(8,128)}, u32[]{:S(2)}) copy-start(f32[2048,64]{0,1:T(8,128)} %slice.334) | copy-start | bytes 1572868
  65.9 3.0 %copy-start.1 = (f32[2048,64]{0,1:T(8,128)S(1)}, f32[2048,64]{0,1:T(8,128)}, u32[]{:S(2)}) copy-start(f32[2048,64]{0,1:T(8,128)} %slice.333) | copy-start | bytes 1572868
  75.0 1.2 copy-start.2
  75.0 1.4 copy-start.3
  86.2 44.7 %all-to-all-start.4 = ((f32[64,2,2048]{2,1,0:T(2,128)}), f32[64,2,2048]{2,1,0:T(2,128)}, u32[]{:S(2)}, u32[]{:S(2)}) async-start(f32[64,2,2048]{2,1,0:T(2,128)} %broadcast_in_dim.29), calls=%async_computation.4 | async-start | bytes 2097152 | tf_op jit(solution)/shard_map/all_to_all | solution.py:60
